TPU v7x, 32 devices: a whole 2x2x4 slice. The times are simulated.
32 devices in a mesh: ep: 4 (over y, x), tp: 8 (over z, core).
Axes of the slice: x: 2, y: 2, z: 4, core: 2. Of those that a mesh axis runs over, the one named last changes fastest.
Arguments:
- tokens: bfloat16 [512, 2048], P('ep'), may hold values from -6 to 6
- conv_state: bfloat16 [512, 3, 2048], P('ep', None, 'tp'), may hold values from -6 to 6
- rec_state: float32 [512, 2048], P('ep', 'tp'), may hold values from -6 to 6
- gate_proj: bfloat16 [2048, 2048], P(None, 'tp'), may hold values from -0.125 to 0.125
- input_proj: bfloat16 [2048, 2048], P(None, 'tp'), may hold values from -0.125 to 0.125
- conv_taps: bfloat16 [4, 2048], P(None, 'tp'), may hold values from -3 to 3
- decay_blocks: bfloat16 [16, 128, 128], P('tp'), may hold values from -0.5 to 0.5
- input_blocks: bfloat16 [16, 128, 128], P('tp'), may hold values from -0.5 to 0.5
- decay_param: float32 [2048], P('tp'), may hold values from 0 to 6
- out_proj: bfloat16 [2048, 2048], P('tp'), may hold values from -0.125 to 0.125
- first_gain: float32 [2048], replicated, may hold values from 0.1 to 1.9
- expert_gate: bfloat16 [4, 2048, 7168], P('ep', None, 'tp'), may hold values from -0.125 to 0.125
- expert_up: bfloat16 [4, 2048, 7168], P('ep', None, 'tp'), may hold values from -0.125 to 0.125
- expert_down: bfloat16 [4, 7168, 2048], P('ep', 'tp'), may hold values from -0.0625 to 0.0625
- routing: int32 [512, 2], P('ep'), may hold values from 0 to 3, all different within a row; in each aligned block of 128 rows (0 to 127, 128 to 255, ...) at most 128 rows name the same one
- route_weight: float32 [512, 2], P('ep'), may hold values from 0.1 to 1
- dense_gate: bfloat16 [2048, 2048], P(None, 'tp'), may hold values from -0.125 to 0.125
- dense_up: bfloat16 [2048, 2048], P(None, 'tp'), may hold values from -0.125 to 0.125
- dense_down: bfloat16 [2048, 2048], P('tp'), may hold values from -0.125 to 0.125
- mix_weight: bfloat16 [2048], replicated, may hold values from -0.125 to 0.125
- second_gain: float32 [2048], P('tp'), may hold values from 0.1 to 1.9
Outputs:
- layer_out: bfloat16 [512, 2048], P('ep', 'tp')
- new_state: float32 [512, 2048], P('ep', 'tp')
- new_conv: bfloat16 [512, 3, 2048], P('ep', None, 'tp')
Inputs may be any that keep to these rules, and one draw needn't show every extreme that they name: `routing`: each row names 2 different experts; in each aligned block of 128 rows (the rows of one index of ep) no expert is named by more than 128 rows, a bound that some expert reaches in some block.
All inputs are finite; a program needn't handle non-finite values.
Results may differ from a plain program's by a relative error of at most 0.013.
Values may be sent and summed in bfloat16 or wider, within the bound.
A program may use at most 64 MiB of HBM per device.

v0:
```python
import jax
import jax.numpy as jnp
from jax import lax
from jax.sharding import PartitionSpec as P

D = 2048
TOPK = 2
ALPHA = 8.0**0.25
RATE_SCALE = 8.0
NORM_EPS = 1e-05


def norm_rows(values, gain_vec):
    centre = values - jnp.mean(values, axis=-1, keepdims=True)
    spread = jnp.mean(centre * centre, axis=-1, keepdims=True)
    return centre * lax.rsqrt(spread + NORM_EPS) * gain_vec


def on_device(
    tokens,
    conv_state,
    rec_state,
    gate_proj,
    input_proj,
    conv_taps,
    decay_blocks,
    input_blocks,
    decay_param,
    out_proj,
    first_gain,
    expert_gate,
    expert_up,
    expert_down,
    routing,
    route_weight,
    dense_gate,
    dense_up,
    dense_down,
    mix_weight,
    second_gain,
):
    count_rows = tokens.shape[0]
    gated = jnp.dot(tokens, gate_proj, preferred_element_type=jnp.float32).astype(jnp.bfloat16)
    inputs = jnp.dot(tokens, input_proj, preferred_element_type=jnp.float32).astype(jnp.bfloat16)
    window = jnp.concatenate([conv_state, inputs[:, None, :]], axis=1)
    convolved = jnp.sum(
        window.astype(jnp.float32) * conv_taps.astype(jnp.float32)[None], axis=1
    ).astype(jnp.bfloat16)
    local_heads = decay_blocks.shape[0]
    heads_view = convolved.reshape(count_rows, local_heads, -1)
    recur_gate = jax.nn.sigmoid(
        jnp.einsum("bhi,hij->bhj", heads_view, decay_blocks, preferred_element_type=jnp.float32)
    ).reshape(count_rows, -1)
    input_gate = jax.nn.sigmoid(
        jnp.einsum("bhi,hij->bhj", heads_view, input_blocks, preferred_element_type=jnp.float32)
    ).reshape(count_rows, -1)
    log_decay = -RATE_SCALE * recur_gate * jax.nn.softplus(-decay_param)
    new_state = jnp.exp(log_decay) * rec_state + jnp.sqrt(
        -jnp.expm1(2.0 * log_decay)
    ) * input_gate * convolved.astype(jnp.float32)
    mixed_rows = (new_state * jax.nn.gelu(gated.astype(jnp.float32), approximate=True)).astype(
        jnp.bfloat16
    )
    partial_mix = jnp.dot(mixed_rows, out_proj, preferred_element_type=jnp.float32)
    mixed = lax.psum(partial_mix.astype(jnp.bfloat16), "tp").astype(jnp.float32)
    normed = norm_rows(ALPHA * tokens.astype(jnp.float32) + mixed, first_gain).astype(jnp.bfloat16)
    tp_index = lax.axis_index("tp")
    tp_count = lax.axis_size("tp")
    own_width = D // tp_count
    own_normed = lax.dynamic_slice_in_dim(normed, tp_index * own_width, own_width, 1)
    local_experts = expert_gate.shape[0]
    ep_count = lax.axis_size("ep")
    experts = local_experts * ep_count
    capacity = max(2, 2 * count_rows * TOPK // experts)
    flat_routes = routing.reshape(-1)
    labels = jnp.arange(experts, dtype=jnp.int32)
    onehot = (flat_routes[:, None] == labels[None, :]).astype(jnp.int32)
    earlier = jnp.cumsum(onehot, axis=0) - onehot
    slot_index = jnp.sum(earlier * onehot, axis=1)
    target = flat_routes * capacity + slot_index
    placed = (target[:, None] == jnp.arange(experts * capacity, dtype=jnp.int32)[None, :]).astype(
        jnp.bfloat16
    )
    token_slots = jnp.sum(placed.reshape(count_rows, TOPK, experts * capacity), axis=1)
    dispatch = jnp.dot(token_slots.T, normed, preferred_element_type=jnp.float32).astype(
        jnp.bfloat16
    )
    arrived = lax.all_to_all(
        dispatch.reshape(experts, capacity, D), "ep", split_axis=0, concat_axis=1, tiled=True
    )
    gate_val = jnp.einsum("erd,edf->erf", arrived, expert_gate, preferred_element_type=jnp.float32)
    up_val = jnp.einsum("erd,edf->erf", arrived, expert_up, preferred_element_type=jnp.float32)
    hidden = (jax.nn.silu(gate_val) * up_val).astype(jnp.bfloat16)
    partial_out = jnp.einsum(
        "erf,efd->erd", hidden, expert_down, preferred_element_type=jnp.float32
    )
    reduced = lax.psum_scatter(
        partial_out.astype(jnp.bfloat16), "tp", scatter_dimension=2, tiled=True
    )
    returned = lax.all_to_all(reduced, "ep", split_axis=1, concat_axis=0, tiled=True)
    returned = returned.reshape(experts * capacity, own_width)
    picked = jnp.dot(placed, returned, preferred_element_type=jnp.float32).reshape(
        count_rows, TOPK, own_width
    )
    routed_sum = jnp.sum(route_weight[:, :, None] * picked, axis=1)
    dense_g = jnp.dot(normed, dense_gate, preferred_element_type=jnp.float32)
    dense_u = jnp.dot(normed, dense_up, preferred_element_type=jnp.float32)
    dense_hidden = (jax.nn.silu(dense_g) * dense_u).astype(jnp.bfloat16)
    dense_part = jnp.dot(dense_hidden, dense_down, preferred_element_type=jnp.float32)
    dense_out = lax.psum_scatter(
        dense_part.astype(jnp.bfloat16), "tp", scatter_dimension=1, tiled=True
    ).astype(jnp.float32)
    mix = jax.nn.sigmoid(jnp.dot(normed, mix_weight, preferred_element_type=jnp.float32))
    combined = ALPHA * own_normed.astype(jnp.float32) + routed_sum + mix[:, None] * dense_out
    row_total, row_square = lax.psum(
        (jnp.sum(combined, axis=1), jnp.sum(combined * combined, axis=1)), "tp"
    )
    row_mean = row_total / D
    row_var = row_square / D - row_mean * row_mean
    layer_out = (
        (combined - row_mean[:, None]) * lax.rsqrt(row_var[:, None] + NORM_EPS) * second_gain
    ).astype(jnp.bfloat16)
    return (layer_out, new_state, window[:, 1:])


def solution(mesh):
    return jax.shard_map(
        on_device,
        mesh=mesh,
        in_specs=(
            P("ep", None),
            P("ep", None, "tp"),
            P("ep", "tp"),
            P(None, "tp"),
            P(None, "tp"),
            P(None, "tp"),
            P("tp", None, None),
            P("tp", None, None),
            P("tp"),
            P("tp", None),
            P(),
            P("ep", None, "tp"),
            P("ep", None, "tp"),
            P("ep", "tp", None),
            P("ep", None),
            P("ep", None),
            P(None, "tp"),
            P(None, "tp"),
            P("tp", None),
            P(),
            P("tp"),
        ),
        out_specs=(P("ep", "tp"), P("ep", "tp"), P("ep", None, "tp")),
        check_vma=False,
    )
```

profile of v0, /device:TPU:0, one launch (start us, length us, event | category | flops | bytes accessed | tf_op | source)
XLA Modules:
  0.0 208.7 jit_solution(3627572307212594813)
XLA Ops:
  7.3 0.8 convert_element_type.84
  8.0 1.8 fusion.23
  9.8 1.0 multiply_reduce_fusion.1
  10.8 1.1 fusion.20
  12.6 1.6 convolution_convert_fusion.2
  14.7 1.2 reduce-window.6
  16.7 56.9 %all-reduce.3.cloned.1.call-done = bf16[128,2048]{1,0:T(8,128)(2,1)} async-done(((bf16[128,2048]{1,0:T(8,128)(2,1)}), bf16[128,2048]{1,0:T(8,128)(2,1)}) %all-reduce.3.cloned.1.call-update) | async-done | bytes 524304 | tf_op jit(solution)/shard_map/psum | solution.py:65
  73.6 1.4 fusion.30
  75.0 1.4 multiply_reduce_fusion
  77.4 27.3 %all_to_all.8 = bf16[4,128,2048]{2,1,0:T(8,128)(2,1)S(1)} all-to-all(bf16[4,128,2048]{2,1,0:T(8,128)(2,1)S(1)} %bitcast.100), channel_id=1, replica_groups=mesh['ep'=4,'tp'=8] {'ep'}, dimensions={0} | all-to-all | bytes 4194304 | tf_op jit(solution)/shard_map/all_to_all | solution.py:88
  104.7 1.3 copy-done.3
  106.0 3.6 %fusion.4 = f32[512,896]{1,0:T(8,128)} fusion(bf16[512,2048]{1,0:T(8,128)(2,1)S(1)} %bitcast.101, bf16[1,2048,896]{2,1,0:T(8,128)(2,1)S(1)} %copy-done.14), kind=kOutput, calls=%fused_computation.4 | convolution fusion | flops 1879048192 | bytes 7602176 | tf_op jit(solution)/shard_map/erd,edf->erf/dot_general | solution.py:91
  109.6 10.2 %fusion.9 = bf16[1,512,2048]{2,1,0:T(8,128)(2,1)} fusion(bf16[1,896,2048]{2,1,0:T(8,128)(2,1)} %param.34, f32[512,896]{1,0:T(8,128)} %fusion.4, bf16[512,2048]{1,0:T(8,128)(2,1)} %bitcast.102, bf16[1,2048,896]{2,1,0:T(8,128)(2,1)} %param.33), kind=kOutput, calls=%fused_computation.8 | convolution fusion | flops 3761897472 | bytes 13369344 | tf_op jit(solution)/shard_map/erf,efd->erd/dot_general | solution.py:94
  119.9 1.6 fusion.73
  121.5 2.8 %convolution_convert_fusion.1 = bf16[128,2048]{1,0:T(8,128)(2,1)} fusion(bf16[256,2048]{1,0:T(8,128)(2,1)S(1)} %copy-done.5, bf16[128,2048]{1,0:T(8,128)(2,1)S(1)} %multiply_convert_fusion.1, bf16[2048,256]{1,0:T(8,128)(2,1)} %param.38, f32[128,256]{1,0:T(8,128)S(1)} %fusion.73), kind=kOutput, calls=%fused_computation.9 | convolution fusion | flops 268894208 | bytes 3276800 | tf_op jit(solution)/shard_map/dot_general | solution.py:109
  125.1 29.4 %reduce-scatter.3.cloned.1.call-done = bf16[1,512,256]{2,1,0:T(8,128)(2,1)} async-done(((bf16[1,512,2048]{2,1,0:T(8,128)(2,1)}), bf16[1,512,256]{2,1,0:T(8,128)(2,1)}) %reduce-scatter.3.cloned.1.call-update) | async-done | bytes 262160 | tf_op jit(solution)/shard_map/reduce_scatter | solution.py:97
  154.6 1.4 copy.120
  156.4 2.2 %reduce.1 = bf16[512,256]{1,0:T(8,128)(2,1)S(1)} reduce(bf16[512,1,256]{2,1,0:T(2,128)(2,1)S(1)} %bitcast.103, bf16[]{:T(256)} %broadcast.115), dimensions={1}, to_apply=%bitcast.99.reduce_sub_computation | reduce | bytes 524290
  158.7 0.8 reshape.150
  159.4 3.7 %all-to-all-start.1 = ((bf16[4,2,16384]{2,1,0:T(2,128)(2,1)}), bf16[4,2,16384]{2,1,0:T(2,128)(2,1)S(1)}, u32[]{:S(2)}, u32[]{:S(2)}) async-start(bf16[4,2,16384]{2,1,0:T(2,128)(2,1)} %reshape.150), calls=%async_computation.2 | async-start | bytes 524288 | tf_op jit(solution)/shard_map/all_to_all | solution.py:100
  163.3 5.1 %all-to-all-done.1 = bf16[4,2,16384]{2,1,0:T(2,128)(2,1)S(1)} async-done(((bf16[4,2,16384]{2,1,0:T(2,128)(2,1)}), bf16[4,2,16384]{2,1,0:T(2,128)(2,1)S(1)}, u32[]{:S(2)}, u32[]{:S(2)}) %all-to-all-start.1) | async-done | bytes 262176 | tf_op jit(solution)/shard_map/all_to_all | solution.py:100
  169.0 17.6 %reduce-scatter.5.cloned.1.call-done = bf16[128,256]{1,0:T(8,128)(2,1)} async-done(((bf16[128,2048]{1,0:T(8,128)(2,1)}), bf16[128,256]{1,0:T(8,128)(2,1)}) %reduce-scatter.5.cloned.1.call-update) | async-done | bytes 65552 | tf_op jit(solution)/shard_map/reduce_scatter | solution.py:110
  186.7 1.0 fusion.72
  187.7 13.7 %all-reduce = (f32[128]{0:T(128)S(1)}, f32[128]{0:T(128)S(1)}) all-reduce(f32[128]{0:T(128)S(1)} %get-tuple-element.4, f32[128]{0:T(128)S(1)} %get-tuple-element.3), channel_id=1, replica_groups=mesh['ep'=4,'tp'=8] {'tp'}, use_global_device_ids=true, to_apply=%region_14.15 | all-reduce | flops 256 | bytes 2048 | tf_op jit(solution)/shard_map/psum | solution.py:115
  (71 shorter events, 5.7 us)
Async XLA Ops:
  7.2 5.4 %copy-start = (bf16[256,2048]{1,0:T(8,128)(2,1)S(1)}, bf16[256,2048]{1,0:T(8,128)(2,1)}, u32[]{:S(2)}) copy-start(bf16[256,2048]{1,0:T(8,128)(2,1)} %param.30) | copy-start | bytes 3145732
  7.2 4.8 %copy-start.15 = (bf16[2,128,128]{2,1,0:T(8,128)(2,1)S(1)}, bf16[2,128,128]{2,1,0:T(8,128)(2,1)}, u32[]{:S(2)}) copy-start(bf16[2,128,128]{2,1,0:T(8,128)(2,1)} %param.28) | copy-start | bytes 196612
  7.2 5.2 %copy-start.13 = (f32[256]{0:T(256)S(1)}, f32[256]{0:T(256)}, u32[]{:S(2)}) copy-start(f32[256]{0:T(256)} %param.29) | copy-start | bytes 3076
  7.2 5.2 %copy-start.8 = (f32[128,256]{1,0:T(8,128)S(1)}, f32[128,256]{1,0:T(8,128)}, u32[]{:S(2)}) copy-start(f32[128,256]{1,0:T(8,128)} %param.23) | copy-start | bytes 393220
  7.2 66.4 %all-reduce.3.cloned.1.call-start = ((), (), s32[]{:S(2)}) async-start(), calls=%async_computation.4 | async-start | bytes 1048576 | tf_op jit(solution)/shard_map/psum | solution.py:65
  8.0 4.5 %copy-start.1 = (bf16[128,2048]{1,0:T(8,128)(2,1)S(1)}, bf16[128,2048]{1,0:T(8,128)(2,1)}, u32[]{:S(2)}) copy-start(bf16[128,2048]{1,0:T(8,128)(2,1)} %param.21) | copy-start | bytes 1572868
  8.0 4.5 %copy-start.4 = (bf16[2048,256]{1,0:T(8,128)(2,1)S(1)}, bf16[2048,256]{1,0:T(8,128)(2,1)}, u32[]{:S(2)}) copy-start(bf16[2048,256]{1,0:T(8,128)(2,1)} %param.24) | copy-start | bytes 3145732
  12.4 1.9 copy-start.10
  12.6 4.0 %copy-start.7 = (f32[128,256]{1,0:T(8,128)}, f32[128,256]{1,0:T(8,128)S(1)}, u32[]{:S(2)}) copy-start(f32[128,256]{1,0:T(8,128)S(1)} %multiply_add_fusion.1) | copy-start | bytes 393220
  14.2 62.2 %copy-start.9 = (f32[2048]{0:T(1024)S(1)}, f32[2048]{0:T(1024)}, u32[]{:S(2)}) copy-start(f32[2048]{0:T(1024)} %param.31) | copy-start | bytes 24580
  14.2 140.3 %reduce-scatter.3.cloned.1.call-start = ((), (), s32[]{:S(2)}) async-start(), calls=%async_computation.5 | async-start | bytes 2359296 | tf_op jit(solution)/shard_map/reduce_scatter | solution.py:97
  73.6 2.8 %copy-start.2 = (bf16[128,2048]{1,0:T(8,128)(2,1)S(1)}, bf16[128,2048]{1,0:T(8,128)(2,1)}, u32[]{:S(2)}) copy-start(bf16[128,2048]{1,0:T(8,128)(2,1)} %all-reduce.3.cloned.1.call-done) | copy-start | bytes 1572868
  77.4 28.6 %copy-start.14 = (bf16[1,2048,896]{2,1,0:T(8,128)(2,1)S(1)}, bf16[1,2048,896]{2,1,0:T(8,128)(2,1)}, u32[]{:S(2)}) copy-start(bf16[1,2048,896]{2,1,0:T(8,128)(2,1)} %param.32) | copy-start | bytes 11010052
  104.7 1.3 copy-start.3
  119.8 1.7 copy-start.5
  119.8 66.8 %reduce-scatter.5.cloned.1.call-start = ((), (), s32[]{:S(2)}) async-start(), calls=%async_computation.6 | async-start | bytes 589824 | tf_op jit(solution)/shard_map/reduce_scatter | solution.py:110
  121.5 2.9 %copy-start.11 = (bf16[2048]{0:T(1024)(128)(2,1)S(1)}, bf16[2048]{0:T(1024)(128)(2,1)}, u32[]{:S(2)}) copy-start(bf16[2048]{0:T(1024)(128)(2,1)} %param.40) | copy-start | bytes 12292
  121.5 2.9 %copy-start.6 = (bf16[128,3,256]{2,0,1:T(8,128)(2,1)S(1)}, bf16[128,3,256]{2,0,1:T(8,128)(2,1)}, u32[]{:S(2)}) copy-start(bf16[128,3,256]{2,0,1:T(8,128)(2,1)} %param.22) | copy-start | bytes 589828
  124.4 44.3 %copy-start.16 = (f32[128,2]{0,1:T(2,128)S(1)}, f32[128,2]{0,1:T(2,128)}, u32[]{:S(2)}) copy-start(f32[128,2]{0,1:T(2,128)} %param.36) | copy-start | bytes 3076
  156.4 45.0 %copy-start.12 = (f32[256]{0:T(256)S(1)}, f32[256]{0:T(256)}, u32[]{:S(2)}) copy-start(f32[256]{0:T(256)} %param.41) | copy-start | bytes 3076
  159.4 9.0 %all-to-all-start.1 = ((bf16[4,2,16384]{2,1,0:T(2,128)(2,1)}), bf16[4,2,16384]{2,1,0:T(2,128)(2,1)S(1)}, u32[]{:S(2)}, u32[]{:S(2)}) async-start(bf16[4,2,16384]{2,1,0:T(2,128)(2,1)} %reshape.150), calls=%async_computation.2 | async-start | bytes 524288 | tf_op jit(solution)/shard_map/all_to_all | solution.py:100
Sparse Core Ops, SparseCore 0:
  14.3 59.2 all-reduce.2
  119.9 34.5 reduce-scatter.2
  156.8 29.8 reduce-scatter.4
where the time goes:
time: 209 us
  waiting for transfers between devices  109 us (52%)
  blocking collectives  41 us (20%)
  matrix products  24.2 us (12%)
  between operations  14.1 us (7%)
  other arithmetic  11.1 us (5%)
  local copies, waits for them, and re-layouts  5.33 us (3%)
  starting transfers between devices  3.79 us (2%)
    psum x1, waiting for transfers between devices, on_device(): mixed = lax.psum(partial_mix.astype(jnp.bfloat16), 'tp').astype(jnp.float32)  56.9 us
    reduce_scatter x1, waiting for transfers between devices, on_device(): lax.psum_scatter(partial_out.astype(jnp.bfloat16), 'tp', scatter_dimensio...  29.4 us
    all_to_all x1, blocking collectives, on_device(): lax.all_to_all(dispatch.reshape(experts, capacity, D), 'ep', split_axis=0...  27.3 us
    reduce_scatter x1, waiting for transfers between devices, on_device(): lax.psum_scatter(dense_part.astype(jnp.bfloat16), 'tp', scatter_dimension...  17.6 us
    psum x1, blocking collectives, on_device(): lax.psum((jnp.sum(combined, axis=1), jnp.sum(combined * combined, axis=1)...  13.7 us
    dot_general x1, matrix products, on_device(): jnp.einsum('erf,efd->erd', hidden, expert_down, preferred_element_type=jn...  10.2 us
    all_to_all x1, waiting for transfers between devices, on_device(): lax.all_to_all(reduced, 'ep', split_axis=1, concat_axis=0, tiled=True)  5.13 us
  transfers between devices with their start and end apart: 4, of which 4 were waited for; matrix products, arithmetic and copies ran while one was open for 6% of the time, Pallas kernels for 0%

commit v1 on v0

--- a/solution.py
+++ b/solution.py
@@ -62,7 +62,9 @@
         jnp.bfloat16
     )
     partial_mix = jnp.dot(mixed_rows, out_proj, preferred_element_type=jnp.float32)
-    mixed = lax.psum(partial_mix.astype(jnp.bfloat16), "tp").astype(jnp.float32)
+    mixed = jnp.sum(lax.all_gather(partial_mix.astype(jnp.bfloat16), axis_name="tp"), 0).astype(
+        jnp.float32
+    )
     normed = norm_rows(ALPHA * tokens.astype(jnp.float32) + mixed, first_gain).astype(jnp.bfloat16)
     tp_index = lax.axis_index("tp")
     tp_count = lax.axis_size("tp")

time: 209 us -> 202 us (0.967)
  waiting for transfers between devices: 109 us -> 98.3 us
  blocking collectives: 41 us -> 43.2 us
    psum x1 -> x0, waiting for transfers between devices: 56.9 us -> none  [on_device(): mixed = lax.psum(partial_mix.astype(jnp.bfloat16), 'tp').astype(jnp.float32)]
    all_gather x0 -> x1, waiting for transfers between devices: none -> 47.3 us  [on_device(): lax.all_gather(partial_mix.astype(jnp.bfloat16), axis_name='tp')]
    reduce_sum x0 -> x1, other arithmetic: none -> 2.95 us  [on_device(): jnp.sum(lax.all_gather(partial_mix.astype(jnp.bfloat16), axis_name='tp'), 0)]
    all_to_all x1, blocking collectives: 27.3 us -> 29.5 us  [on_device(): lax.all_to_all(dispatch.reshape(experts, capacity, D), 'ep', split_axis=0...]
  transfers between devices with their start and end apart: 4 -> 4, of which waited for: 4 -> 4; matrix products, arithmetic and copies ran while one was open for 6% -> 7% of each run, Pallas kernels for 0% -> 0%
where the time goes in v1:
time: 202 us; the launch traced here: 201 us
  waiting for transfers between devices  98.3 us (49%)
  blocking collectives  43.2 us (21%)
  matrix products  24.2 us (12%)
  between operations  14.1 us (7%)
  other arithmetic  11.9 us (6%)
  local copies, waits for them, and re-layouts  5.42 us (3%)
  starting transfers between devices  3.95 us (2%)
    all_gather x1, waiting for transfers between devices, on_device(): lax.all_gather(partial_mix.astype(jnp.bfloat16), axis_name='tp')  47.3 us
    all_to_all x1, blocking collectives, on_device(): lax.all_to_all(dispatch.reshape(experts, capacity, D), 'ep', split_axis=0...  29.5 us
    reduce_scatter x1, waiting for transfers between devices, on_device(): lax.psum_scatter(partial_out.astype(jnp.bfloat16), 'tp', scatter_dimensio...  28 us
    reduce_scatter x1, waiting for transfers between devices, on_device(): lax.psum_scatter(dense_part.astype(jnp.bfloat16), 'tp', scatter_dimension...  17.8 us
    psum x1, blocking collectives, on_device(): lax.psum((jnp.sum(combined, axis=1), jnp.sum(combined * combined, axis=1)...  13.8 us
    dot_general x1, matrix products, on_device(): jnp.einsum('erf,efd->erd', hidden, expert_down, preferred_element_type=jn...  10.2 us
    all_to_all x1, waiting for transfers between devices, on_device(): lax.all_to_all(reduced, 'ep', split_axis=1, concat_axis=0, tiled=True)  5.13 us
  transfers between devices with their start and end apart: 4, of which 4 were waited for; matrix products, arithmetic and copies ran while one was open for 7% of the time, Pallas kernels for 0%

profile of v1, /device:TPU:0, one launch (start us, length us, event | category | flops | bytes accessed | tf_op | source)
XLA Modules:
  0.0 201.1 jit_solution(11750110382440669874)
XLA Ops:
  7.3 0.8 convert_element_type.86
  8.0 1.8 fusion.23
  9.8 1.0 multiply_reduce_fusion.1
  10.8 1.1 fusion.20
  12.6 1.6 convolution_convert_fusion.2
  14.7 1.2 reduce-window.6
  16.7 47.3 %all-gather.3.cloned.1.call-done = bf16[1024,2048]{1,0:T(8,128)(2,1)} async-done(((bf16[128,2048]{1,0:T(8,128)(2,1)}), bf16[1024,2048]{1,0:T(8,128)(2,1)}) %all-gather.3.cloned.1.call-update) | async-done | bytes 4194320 | tf_op jit(solution)/shard_map/all_gather | solution.py:65
  64.0 3.0 %reduce_sum.90 = bf16[128,2048]{1,0:T(8,128)(2,1)S(1)} reduce(bf16[8,128,2048]{2,1,0:T(8,128)(2,1)} %bitcast.102, bf16[]{:T(256)} %constant.24.clone.1), dimensions={0}, to_apply=%region_1.2 | reduce | flops 1835008 | bytes 4718594 | tf_op jit(solution)/shard_map/reduce_sum | solution.py:65
  68.7 29.5 %all_to_all.8 = bf16[4,128,2048]{2,1,0:T(8,128)(2,1)S(1)} all-to-all(bf16[4,128,2048]{2,1,0:T(8,128)(2,1)S(1)} %bitcast.101), channel_id=1, replica_groups=mesh['ep'=4,'tp'=8] {'ep'}, dimensions={0} | all-to-all | bytes 4194304 | tf_op jit(solution)/shard_map/all_to_all | solution.py:90
  98.1 1.3 copy-done.2
  99.4 3.6 %fusion.4 = f32[512,896]{1,0:T(8,128)} fusion(bf16[512,2048]{1,0:T(8,128)(2,1)S(1)} %bitcast.103, bf16[1,2048,896]{2,1,0:T(8,128)(2,1)S(1)} %copy-done.13), kind=kOutput, calls=%fused_computation.4 | convolution fusion | flops 1879048192 | bytes 7602176 | tf_op jit(solution)/shard_map/erd,edf->erf/dot_general | solution.py:93
  103.0 10.2 %fusion.9 = bf16[1,512,2048]{2,1,0:T(8,128)(2,1)} fusion(bf16[1,896,2048]{2,1,0:T(8,128)(2,1)} %param.34, f32[512,896]{1,0:T(8,128)} %fusion.4, bf16[512,2048]{1,0:T(8,128)(2,1)} %bitcast.104, bf16[1,2048,896]{2,1,0:T(8,128)(2,1)} %param.33), kind=kOutput, calls=%fused_computation.8 | convolution fusion | flops 3761897472 | bytes 13369344 | tf_op jit(solution)/shard_map/erf,efd->erd/dot_general | solution.py:96
  113.5 1.6 fusion.73
  115.1 2.8 %convolution_convert_fusion.1 = bf16[128,2048]{1,0:T(8,128)(2,1)} fusion(bf16[256,2048]{1,0:T(8,128)(2,1)S(1)} %copy-done.4, bf16[128,2048]{1,0:T(8,128)(2,1)S(1)} %multiply_convert_fusion.1, bf16[2048,256]{1,0:T(8,128)(2,1)} %param.38, f32[128,256]{1,0:T(8,128)S(1)} %fusion.73), kind=kOutput, calls=%fused_computation.9 | convolution fusion | flops 268894208 | bytes 3276800 | tf_op jit(solution)/shard_map/dot_general | solution.py:111
  118.7 28.0 %reduce-scatter.3.cloned.1.call-done = bf16[1,512,256]{2,1,0:T(8,128)(2,1)} async-done(((bf16[1,512,2048]{2,1,0:T(8,128)(2,1)}), bf16[1,512,256]{2,1,0:T(8,128)(2,1)}) %reduce-scatter.3.cloned.1.call-update) | async-done | bytes 262160 | tf_op jit(solution)/shard_map/reduce_scatter | solution.py:99
  146.8 1.4 copy.120
  148.6 2.2 %reduce.2 = bf16[512,256]{1,0:T(8,128)(2,1)S(1)} reduce(bf16[512,1,256]{2,1,0:T(2,128)(2,1)S(1)} %bitcast.105, bf16[]{:T(256)} %broadcast.115), dimensions={1}, to_apply=%bitcast.100.reduce_sub_computation | reduce | bytes 524290
  150.9 0.8 reshape.151
  151.6 3.6 %all-to-all-start.1 = ((bf16[4,2,16384]{2,1,0:T(2,128)(2,1)}), bf16[4,2,16384]{2,1,0:T(2,128)(2,1)S(1)}, u32[]{:S(2)}, u32[]{:S(2)}) async-start(bf16[4,2,16384]{2,1,0:T(2,128)(2,1)} %reshape.151), calls=%async_computation.2 | async-start | bytes 524288 | tf_op jit(solution)/shard_map/all_to_all | solution.py:102
  155.5 5.1 %all-to-all-done.1 = bf16[4,2,16384]{2,1,0:T(2,128)(2,1)S(1)} async-done(((bf16[4,2,16384]{2,1,0:T(2,128)(2,1)}), bf16[4,2,16384]{2,1,0:T(2,128)(2,1)S(1)}, u32[]{:S(2)}, u32[]{:S(2)}) %all-to-all-start.1) | async-done | bytes 262176 | tf_op jit(solution)/shard_map/all_to_all | solution.py:102
  161.2 17.8 %reduce-scatter.5.cloned.1.call-done = bf16[128,256]{1,0:T(8,128)(2,1)} async-done(((bf16[128,2048]{1,0:T(8,128)(2,1)}), bf16[128,256]{1,0:T(8,128)(2,1)}) %reduce-scatter.5.cloned.1.call-update) | async-done | bytes 65552 | tf_op jit(solution)/shard_map/reduce_scatter | solution.py:112
  179.0 1.0 fusion.72
  180.0 13.8 %all-reduce = (f32[128]{0:T(128)S(1)}, f32[128]{0:T(128)S(1)}) all-reduce(f32[128]{0:T(128)S(1)} %get-tuple-element.4, f32[128]{0:T(128)S(1)} %get-tuple-element.3), channel_id=1, replica_groups=mesh['ep'=4,'tp'=8] {'tp'}, use_global_device_ids=true, to_apply=%region_14.15 | all-reduce | flops 256 | bytes 2048 | tf_op jit(solution)/shard_map/psum | solution.py:117
  193.8 0.7 multiply_convert_fusion.2
  (70 shorter events, 5.9 us)
Async XLA Ops:
  7.2 5.4 %copy-start = (bf16[256,2048]{1,0:T(8,128)(2,1)S(1)}, bf16[256,2048]{1,0:T(8,128)(2,1)}, u32[]{:S(2)}) copy-start(bf16[256,2048]{1,0:T(8,128)(2,1)} %param.30) | copy-start | bytes 3145732
  7.2 4.8 %copy-start.14 = (bf16[2,128,128]{2,1,0:T(8,128)(2,1)S(1)}, bf16[2,128,128]{2,1,0:T(8,128)(2,1)}, u32[]{:S(2)}) copy-start(bf16[2,128,128]{2,1,0:T(8,128)(2,1)} %param.28) | copy-start | bytes 196612
  7.2 5.2 %copy-start.12 = (f32[256]{0:T(256)S(1)}, f32[256]{0:T(256)}, u32[]{:S(2)}) copy-start(f32[256]{0:T(256)} %param.29) | copy-start | bytes 3076
  7.2 5.2 %copy-start.7 = (f32[128,256]{1,0:T(8,128)S(1)}, f32[128,256]{1,0:T(8,128)}, u32[]{:S(2)}) copy-start(f32[128,256]{1,0:T(8,128)} %param.23) | copy-start | bytes 393220
  7.2 56.7 %all-gather.3.cloned.1.call-start = ((), (), s32[]{:S(2)}) async-start(), calls=%async_computation.6 | async-start | bytes 4718592 | tf_op jit(solution)/shard_map/all_gather | solution.py:65
  8.0 4.5 %copy-start.1 = (bf16[128,2048]{1,0:T(8,128)(2,1)S(1)}, bf16[128,2048]{1,0:T(8,128)(2,1)}, u32[]{:S(2)}) copy-start(bf16[128,2048]{1,0:T(8,128)(2,1)} %param.21) | copy-start | bytes 1572868
  8.0 4.5 %copy-start.3 = (bf16[2048,256]{1,0:T(8,128)(2,1)S(1)}, bf16[2048,256]{1,0:T(8,128)(2,1)}, u32[]{:S(2)}) copy-start(bf16[2048,256]{1,0:T(8,128)(2,1)} %param.24) | copy-start | bytes 3145732
  12.4 1.9 copy-start.9
  12.6 4.0 %copy-start.6 = (f32[128,256]{1,0:T(8,128)}, f32[128,256]{1,0:T(8,128)S(1)}, u32[]{:S(2)}) copy-start(f32[128,256]{1,0:T(8,128)S(1)} %multiply_add_fusion.1) | copy-start | bytes 393220
  14.2 132.5 %reduce-scatter.3.cloned.1.call-start = ((), (), s32[]{:S(2)}) async-start(), calls=%async_computation.4 | async-start | bytes 2359296 | tf_op jit(solution)/shard_map/reduce_scatter | solution.py:99
  66.9 0.7 copy-start.8
  68.6 30.8 %copy-start.13 = (bf16[1,2048,896]{2,1,0:T(8,128)(2,1)S(1)}, bf16[1,2048,896]{2,1,0:T(8,128)(2,1)}, u32[]{:S(2)}) copy-start(bf16[1,2048,896]{2,1,0:T(8,128)(2,1)} %param.32) | copy-start | bytes 11010052
  98.1 1.3 copy-start.2
  113.2 1.9 copy-start.4
  113.2 65.7 %reduce-scatter.5.cloned.1.call-start = ((), (), s32[]{:S(2)}) async-start(), calls=%async_computation.5 | async-start | bytes 589824 | tf_op jit(solution)/shard_map/reduce_scatter | solution.py:112
  115.1 2.9 %copy-start.10 = (bf16[2048]{0:T(1024)(128)(2,1)S(1)}, bf16[2048]{0:T(1024)(128)(2,1)}, u32[]{:S(2)}) copy-start(bf16[2048]{0:T(1024)(128)(2,1)} %param.40) | copy-start | bytes 12292
  115.1 2.9 %copy-start.5 = (bf16[128,3,256]{2,0,1:T(8,128)(2,1)S(1)}, bf16[128,3,256]{2,0,1:T(8,128)(2,1)}, u32[]{:S(2)}) copy-start(bf16[128,3,256]{2,0,1:T(8,128)(2,1)} %param.22) | copy-start | bytes 589828
  118.0 42.9 %copy-start.15 = (f32[128,2]{0,1:T(2,128)S(1)}, f32[128,2]{0,1:T(2,128)}, u32[]{:S(2)}) copy-start(f32[128,2]{0,1:T(2,128)} %param.36) | copy-start | bytes 3076
  148.6 45.2 %copy-start.11 = (f32[256]{0:T(256)S(1)}, f32[256]{0:T(256)}, u32[]{:S(2)}) copy-start(f32[256]{0:T(256)} %param.41) | copy-start | bytes 3076
  151.6 9.0 %all-to-all-start.1 = ((bf16[4,2,16384]{2,1,0:T(2,128)(2,1)}), bf16[4,2,16384]{2,1,0:T(2,128)(2,1)S(1)}, u32[]{:S(2)}, u32[]{:S(2)}) async-start(bf16[4,2,16384]{2,1,0:T(2,128)(2,1)} %reshape.151), calls=%async_computation.2 | async-start | bytes 524288 | tf_op jit(solution)/shard_map/all_to_all | solution.py:102
Sparse Core Ops, SparseCore 0:
  14.3 49.5 all-gather.2
  113.3 33.3 reduce-scatter.2
  149.0 29.9 reduce-scatter.4
